TPU v7x, 256 devices: a 4x2x16 block of a 4x16x16 slice. The times are simulated.
256 devices in a mesh: grp: 2 (over y), ep: 32 (over z, core), tp: 4 (over x).
Axes of the slice: x: 4, y: 2, z: 16, core: 2. Of those that a mesh axis runs over, the one named last changes fastest.
The devices are a block of a 4x16x16 slice.
Arguments:
- mixer_input: bfloat16 [32768, 2048], P(('grp', 'ep', 'tp')), parts along dimension 0, may hold values from -8 to 8
- forget_cumsum: float32 [8, 32768], P('tp', 'grp'), parts along dimension 1, may hold values from -2051 to 0, as said below
- mixer_gain: float32 [2048], replicated, may hold values from 0.1 to 1.9
- query_weight: bfloat16 [2048, 1024], P(None, 'tp'), may hold values from -6 to 6
- key_weight: bfloat16 [2048, 1024], P(None, 'tp'), may hold values from -6 to 6
- value_weight: bfloat16 [2048, 1024], P(None, 'tp'), may hold values from -0.125 to 0.125
- out_weight: bfloat16 [1024, 2048], P('tp'), may hold values from -0.1875 to 0.1875
- post_gain: float32 [2048], replicated, may hold values from 0.1 to 1.9
- expert_input: bfloat16 [32768, 2048], P(('grp', 'ep', 'tp')), parts along dimension 0, may hold values from -6 to 6
- expert_gain: float32 [2048], replicated, may hold values from 0.1 to 1.9
- routes: int32 [32768, 2], P(('grp', 'ep', 'tp')), parts along dimension 0, may hold values from 0 to 31, all different within a row; in each aligned block of 128 rows (0 to 127, 128 to 255, ...) at most 9 rows name the same one
- route_weight: float32 [32768, 2], P(('grp', 'ep', 'tp')), parts along dimension 0, may hold values from 0.2 to 1
- expert_gate: bfloat16 [32, 2048, 2048], P('ep', None, 'tp'), may hold values from -0.125 to 0.125
- expert_upward: bfloat16 [32, 2048, 2048], P('ep', None, 'tp'), may hold values from -0.125 to 0.125
- expert_down: bfloat16 [32, 2048, 2048], P('ep', 'tp'), may hold values from -0.125 to 0.125
Outputs:
- mixer_output: bfloat16 [32768, 2048], P(('grp', 'ep', 'tp')), parts along dimension 0
- expert_output: bfloat16 [32768, 2048], P(('grp', 'ep', 'tp')), parts along dimension 0
There are 2 independent parts, one for each index of `grp`. A program takes and returns all parts, laid end to end along the dimension named above; an argument that names none is the same for every part. Nothing has to cross between parts.
Inputs may be any that keep to these rules, and one draw needn't show every extreme that they name: `forget_cumsum`: each head's row never rises along positions. `routes`: A row names 2 different experts. Within the rows of one device (aligned blocks of 128 rows) no expert is named by more than 9 rows, and in every draw some expert is named by exactly 9 rows of some block.
All inputs are finite; a program needn't handle non-finite values.
Results may differ from a plain program's by a relative error of at most 0.012.
Values may be sent and summed in bfloat16 or wider, within the bound.
A program may use at most 128 MiB of HBM per device.

v0:
```python
import jax
import jax.numpy as jnp
from jax import lax
from jax.sharding import PartitionSpec as P

EPS = 1e-06
MASKED = -1e30


def sent_to_all(value, axis):
    copies = jnp.broadcast_to(value, (lax.axis_size(axis), *value.shape))
    return lax.all_to_all(copies, axis, split_axis=0, concat_axis=0, tiled=True)


def joined_along(parts, dim):
    parts = jnp.moveaxis(parts, 0, dim)
    shape = parts.shape
    return parts.reshape(*shape[:dim], shape[dim] * shape[dim + 1], *shape[dim + 2 :])


def gathered_copies(value, axis, dim):
    parts = sent_to_all(value, axis)
    return joined_along(parts, dim)


def in_one_piece(arrays, axis, dim, along):
    widths = [a.shape[along] for a in arrays]
    both = jnp.concatenate(arrays, axis=along)
    whole = lax.all_gather(both, axis, axis=dim, tiled=True)
    return tuple(jnp.split(whole, [sum(widths[:k]) for k in range(1, len(widths))], axis=along))


def cut_along(value, dim, count):
    before, after = (value.shape[:dim], value.shape[dim + 1 :])
    return jnp.moveaxis(value.reshape(*before, count, -1, *after), dim, 0)


def summed_on_arrival(value, axis, dim):
    parts = cut_along(value, dim, lax.axis_size(axis))
    arrived = lax.all_to_all(parts, axis, split_axis=0, concat_axis=0, tiled=True)
    return arrived.astype(jnp.float32).sum(axis=0)


def normalize(row_block, gain):
    values = row_block.astype(jnp.float32)
    inverse = lax.rsqrt(jnp.mean(values * values, axis=-1, keepdims=True) + EPS)
    return values * inverse * gain


def on_device(
    mixer_input,
    forget_cumsum,
    mixer_gain,
    query_weight,
    key_weight,
    value_weight,
    out_weight,
    post_gain,
    expert_input,
    expert_gain,
    routes,
    route_weight,
    expert_gate,
    expert_upward,
    expert_down,
):
    ep_count = lax.axis_size("ep")
    tp_count = lax.axis_size("tp")
    mix_rows = mixer_input.shape[0]
    feature_width = mixer_input.shape[1]
    heads_local = forget_cumsum.shape[0]
    head_width = query_weight.shape[1]
    head_dim = head_width // heads_local
    group_span = mix_rows * tp_count
    first_pos = lax.axis_index("ep") * group_span
    last_pos = first_pos + group_span - 1
    score_scale = head_dim ** (-0.5)
    normed = normalize(mixer_input, mixer_gain).astype(jnp.bfloat16)
    segment = gathered_copies(normed, "tp", 0)
    products = [
        jnp.dot(segment, weight, preferred_element_type=jnp.float32)
        for weight in (query_weight, key_weight, value_weight)
    ]
    joined = jnp.concatenate(products, axis=1).astype(jnp.bfloat16)
    queries = joined[:, :head_width].reshape(group_span, heads_local, head_dim)
    key_rows = joined[:, head_width : 2 * head_width]
    value_rows = joined[:, 2 * head_width :]
    query_pos = first_pos + jnp.arange(group_span, dtype=jnp.int32)
    query_gate = lax.dynamic_slice_in_dim(forget_cumsum, first_pos, group_span, 1)

    def key_block(state, key_part, value_part, key_first):
        key_count = key_part.shape[0]

        def compute(current):
            running_max, running_sum, running_acc = current
            key_heads = key_part.reshape(key_count, heads_local, head_dim)
            value_heads = value_part.reshape(key_count, heads_local, head_dim)
            key_gate = lax.dynamic_slice_in_dim(forget_cumsum, key_first, key_count, 1)
            scores = (
                jnp.einsum("qhd,khd->hqk", queries, key_heads, preferred_element_type=jnp.float32)
                * score_scale
            )
            scores = scores + query_gate[:, :, None] - key_gate[:, None, :]
            key_pos = key_first + jnp.arange(key_count, dtype=jnp.int32)
            visible = (key_pos[None, :] <= query_pos[:, None])[None]
            scores = jnp.where(visible, scores, MASKED)
            new_max = jnp.maximum(running_max, jnp.max(scores, axis=-1))
            weights = jnp.where(visible, jnp.exp(scores - new_max[..., None]), 0.0)
            rescale = jnp.exp(running_max - new_max)
            running_sum = running_sum * rescale + jnp.sum(weights, axis=-1)
            running_acc = running_acc * rescale[..., None] + jnp.einsum(
                "hqk,khd->hqd",
                weights.astype(jnp.bfloat16),
                value_heads,
                preferred_element_type=jnp.float32,
            )
            return (new_max, running_sum, running_acc)

        def keep_state(current):
            return current

        return lax.cond(key_first > last_pos, keep_state, compute, state)

    initial = (
        jnp.full((heads_local, group_span), MASKED, jnp.float32),
        jnp.zeros((heads_local, group_span), jnp.float32),
        jnp.zeros((heads_local, group_span, head_dim), jnp.float32),
    )
    key_part, value_part = in_one_piece((key_rows, value_rows), "ep", 0, 1)
    row_count = key_part.shape[0]
    block_size = 512
    block_count = row_count // block_size

    def advance_increment(block_index, current):
        offset = block_index * block_size
        return key_block(
            current,
            lax.dynamic_slice_in_dim(key_part, offset, block_size, 0),
            lax.dynamic_slice_in_dim(value_part, offset, block_size, 0),
            offset,
        )

    running_max, running_sum, running_acc = lax.fori_loop(
        0, block_count, advance_increment, initial
    )
    attended = (running_acc / running_sum[..., None]).astype(jnp.bfloat16)
    attended = attended.transpose(1, 0, 2).reshape(group_span, head_width)
    moe_rows, top_count = routes.shape
    experts_local = expert_gate.shape[0]
    experts_all = ep_count * experts_local
    capacity = (moe_rows * top_count * 9 + 8 * experts_all - 1) // (8 * experts_all)
    slots_all = experts_all * capacity
    normed_moe = normalize(expert_input, expert_gain).astype(jnp.bfloat16)
    flat_routes = routes.reshape(-1)
    member = (flat_routes[:, None] == jnp.arange(experts_all, dtype=jnp.int32)[None, :]).astype(
        jnp.int32
    )
    before = jnp.cumsum(member, axis=0) - member
    slot_rank = jnp.sum(before * member, axis=1)
    slot_index = (flat_routes * capacity + slot_rank).reshape(moe_rows, top_count)
    slot_ids = jnp.arange(slots_all, dtype=jnp.int32)
    choosers = [
        (slot_index[:, which][:, None] == slot_ids[None, :]).astype(jnp.bfloat16)
        for which in range(top_count)
    ]
    dispatch = choosers[0]
    which = 1
    dispatch = dispatch + choosers[which]
    outgoing = lax.dot_general(
        dispatch, normed_moe, (((0,), (0,)), ((), ())), preferred_element_type=jnp.float32
    ).astype(jnp.bfloat16)
    outgoing = outgoing.reshape(ep_count, experts_local, capacity, feature_width)
    arrived = lax.all_to_all(outgoing, "ep", split_axis=0, concat_axis=0, tiled=True)
    stacked = lax.all_gather(arrived, "tp", axis=0, tiled=True).reshape(
        tp_count, ep_count, experts_local, capacity, feature_width
    )
    shard_axis = 0
    expert_rows_count = ep_count * experts_local * capacity

    def expert_term(block_index):
        selected = lax.dynamic_index_in_dim(stacked, block_index, shard_axis, keepdims=False)
        gate_proj = jnp.einsum(
            "secd,edf->secf", selected, expert_gate, preferred_element_type=jnp.float32
        )
        upward = jnp.einsum(
            "secd,edf->secf", selected, expert_upward, preferred_element_type=jnp.float32
        )
        hidden = (jax.nn.silu(gate_proj) * upward).astype(jnp.bfloat16)
        result = jnp.einsum(
            "secf,efd->secd", hidden, expert_down, preferred_element_type=jnp.float32
        )
        return result.reshape(expert_rows_count, feature_width)

    selected = attended
    mixer_sum = summed_on_arrival(
        jnp.dot(selected, out_weight, preferred_element_type=jnp.float32).astype(jnp.bfloat16),
        "tp",
        0,
    )
    first_block = jnp.int32(0) // expert_rows_count
    pieces = [
        expert_term(first_block + offset)
        for offset in range(expert_rows_count * lax.axis_size("tp") // expert_rows_count)
    ]
    expert_sum = summed_on_arrival(jnp.concatenate(pieces, axis=0).astype(jnp.bfloat16), "tp", 0)
    mixer_output = normalize(mixer_sum, post_gain).astype(jnp.bfloat16)
    results = expert_sum.astype(jnp.bfloat16).reshape(
        ep_count, experts_local, capacity, feature_width
    )
    returned = lax.all_to_all(results, "ep", split_axis=0, concat_axis=0, tiled=True).reshape(
        slots_all, feature_width
    )
    combined = jnp.zeros((moe_rows, feature_width), jnp.float32)
    for which in range(top_count):
        picked = jnp.dot(choosers[which], returned, preferred_element_type=jnp.float32)
        combined = combined + route_weight[:, which : which + 1] * picked
    expert_output = combined.astype(jnp.bfloat16)
    return (mixer_output, expert_output)


def solution(mesh):
    in_specs = (
        P(("grp", "ep", "tp"), None),
        P("tp", "grp"),
        P(),
        P(None, "tp"),
        P(None, "tp"),
        P(None, "tp"),
        P("tp", None),
        P(),
        P(("grp", "ep", "tp"), None),
        P(),
        P(("grp", "ep", "tp"), None),
        P(("grp", "ep", "tp"), None),
        P("ep", None, "tp"),
        P("ep", None, "tp"),
        P("ep", "tp", None),
    )
    out_specs = (P(("grp", "ep", "tp"), None), P(("grp", "ep", "tp"), None))
    return jax.shard_map(
        on_device, mesh=mesh, in_specs=in_specs, out_specs=out_specs, check_vma=False
    )
```

profile of v0, /device:TPU:1953, one launch (start us, length us, event | category | flops | bytes accessed | tf_op | source)
XLA Modules:
  0.0 507.1 jit_solution(11587271823541856930)
XLA Ops:
  14.8 98.5 %all_to_all.25 = bf16[32,1,9,2048]{3,2,1,0:T(8,128)(2,1)S(1)} all-to-all(bf16[32,1,9,2048]{3,2,1,0:T(8,128)(2,1)} %bitcast.285), channel_id=1, replica_groups=mesh['grp'=2,'ep'=32,'tp'=4] {'ep'}, dimensions={0} | all-to-all | bytes 2359296 | tf_op jit(solution)/shard_map/all_to_all | solution.py:173
  115.9 39.8 %all_to_all.26 = bf16[4,128,2048]{2,1,0:T(8,128)(2,1)S(1)} all-to-all(bf16[4,128,2048]{2,1,0:T(8,128)(2,1)S(1)} %broadcast_in_dim.60), channel_id=1, replica_groups=mesh['grp'=2,'ep'=32,'tp'=4] {'tp'}, dimensions={0} | all-to-all | bytes 4194304 | tf_op jit(solution)/shard_map/all_to_all | solution.py:12
  159.4 25.5 %all-gather.5.cloned.1.call-done = bf16[128,1,9,2048]{3,0,2,1:T(8,128)(2,1)} async-done(((bf16[32,1,9,2048]{3,0,2,1:T(8,128)(2,1)}), bf16[128,1,9,2048]{3,0,2,1:T(8,128)(2,1)}) %all-gather.5.cloned.1.call-update) | async-done | bytes 4718608 | tf_op jit(solution)/shard_map/all_gather | solution.py:174
  199.5 4.9 fusion.10
  214.1 4.7 fusion.11
  228.6 4.7 fusion.12
  240.7 5.2 %all-to-all-start.3 = ((bf16[4,288,2048]{2,1,0:T(8,128)(2,1)}), bf16[4,288,2048]{2,1,0:T(8,128)(2,1)}, u32[]{:S(2)}, u32[]{:S(2)}) async-start(bf16[4,288,2048]{2,1,0:T(8,128)(2,1)} %bitcast.284), calls=%async_computation.3 | async-start | bytes 9437184 | tf_op jit(solution)/shard_map/all_to_all | solution.py:40
  248.8 51.1 %all-to-all-done.3 = bf16[4,288,2048]{2,1,0:T(8,128)(2,1)} async-done(((bf16[4,288,2048]{2,1,0:T(8,128)(2,1)}), bf16[4,288,2048]{2,1,0:T(8,128)(2,1)}, u32[]{:S(2)}, u32[]{:S(2)}) %all-to-all-start.3) | async-done | bytes 4718624 | tf_op jit(solution)/shard_map/all_to_all | solution.py:40
  304.8 13.3 %all-to-all-start.4 = ((bf16[32,1,9,2048]{3,2,1,0:T(8,128)(2,1)}), bf16[32,1,9,2048]{3,2,1,0:T(8,128)(2,1)}, u32[]{:S(2)}, u32[]{:S(2)}) async-start(bf16[32,1,9,2048]{3,2,1,0:T(8,128)(2,1)} %bitcast.72), calls=%async_computation.4 | async-start | bytes 4194304 | tf_op jit(solution)/shard_map/all_to_all | solution.py:210
  318.1 11.5 %fusion.154 = (bf16[16384,256]{0,1:T(8,128)(2,1)}, bf16[16384,256]{0,1:T(8,128)(2,1)}) fusion(bf16[16384,512]{0,1:T(8,128)(2,1)} %all-gather.3.cloned.1.call-done), kind=kLoop, calls=%fused_computation.153 | loop fusion | bytes 33554432 | tf_op jit(solution)/shard_map/split | solution.py:30
  329.6 136.1 %while.18 = (s32[]{:T(128)}, f32[2,512]{1,0:T(2,128)S(1)}, f32[2,512]{1,0:T(2,128)S(1)}, f32[2,512,128]{2,1,0:T(8,128)S(1)}, s32[]{:T(128)}, /*index=5*/bf16[163...) while((s32[]{:T(128)}, f32[2,512]{1,0:T(2,128)S(1)}, ...), condition=%wide.region_6.7_spmd.clone, body=%wide.region_1.6_spmd.clone.sunk | while | flops 274729984 | bytes 10318161 | solution.py:143
  338.2 4.2 conditional.3
  346.7 4.2 conditional.3
  359.4 4.2 conditional.3
  367.9 4.2 conditional.3
  380.7 4.2 conditional.3
  402.0 4.2 conditional.3
  410.5 4.2 conditional.3
  423.2 4.2 conditional.3
  431.7 4.2 conditional.3
  444.5 4.2 conditional.3
  453.0 4.2 conditional.3
  469.0 4.7 all-to-all-start.1
  477.3 19.5 %all-to-all-done.1 = bf16[4,128,2048]{2,1,0:T(8,128)(2,1)} async-done(((bf16[4,128,2048]{2,1,0:T(8,128)(2,1)}), bf16[4,128,2048]{2,1,0:T(8,128)(2,1)}, u32[]{:S(2)}, u32[]{:S(2)}) %all-to-all-start.1) | async-done | bytes 2097184 | tf_op jit(solution)/shard_map/all_to_all | solution.py:40
  (459 shorter events, 294.0 us)
Async XLA Ops:
  7.2 181.2 %copy-start = (bf16[1,512,2048]{2,1,0:T(8,128)(2,1)S(1)}, bf16[1,512,2048]{2,1,0:T(8,128)(2,1)}, u32[]{:S(2)}) copy-start(bf16[1,512,2048]{2,1,0:T(8,128)(2,1)} %param.33) | copy-start | bytes 6291460
  7.2 177.6 %all-gather.5.cloned.1.call-start = ((), (), s32[]{:S(2)}) async-start(), calls=%async_computation.6 | async-start | bytes 5898240 | tf_op jit(solution)/shard_map/all_gather | solution.py:174
  113.3 1.9 copy-start.4
  113.3 2.1 copy-start.6
  115.1 203.0 %all-gather.3.cloned.1.call-start = ((), (), s32[]{:S(2)}) async-start(), calls=%async_computation.5 | async-start | bytes 17301504 | tf_op jit(solution)/shard_map/all_gather | solution.py:29
  115.9 39.9 %copy-start.9 = (bf16[2048,256]{1,0:T(8,128)(2,1)S(1)}, bf16[2048,256]{1,0:T(8,128)(2,1)}, u32[]{:S(2)}) copy-start(bf16[2048,256]{1,0:T(8,128)(2,1)} %param.24) | copy-start | bytes 3145732
  155.7 2.8 copy-start.2
  155.7 2.0 copy-start.10
  240.7 5.9 %copy-start.3 = (bf16[4,128,2048]{2,1,0:T(8,128)(2,1)S(1)}, bf16[4,128,2048]{2,1,0:T(8,128)(2,1)}, u32[]{:S(2)}) copy-start(bf16[4,128,2048]{2,1,0:T(8,128)(2,1)} %copy-done.2) | copy-start | bytes 6291460
  240.7 59.2 %all-to-all-start.3 = ((bf16[4,288,2048]{2,1,0:T(8,128)(2,1)}), bf16[4,288,2048]{2,1,0:T(8,128)(2,1)}, u32[]{:S(2)}, u32[]{:S(2)}) async-start(bf16[4,288,2048]{2,1,0:T(8,128)(2,1)} %bitcast.284), calls=%async_computation.3 | async-start | bytes 9437184 | tf_op jit(solution)/shard_map/all_to_all | solution.py:40
  304.8 164.2 %all-to-all-start.4 = ((bf16[32,1,9,2048]{3,2,1,0:T(8,128)(2,1)}), bf16[32,1,9,2048]{3,2,1,0:T(8,128)(2,1)}, u32[]{:S(2)}, u32[]{:S(2)}) async-start(bf16[32,1,9,2048]{3,2,1,0:T(8,128)(2,1)} %bitcast.72), calls=%async_computation.4 | async-start | bytes 4194304 | tf_op jit(solution)/shard_map/all_to_all | solution.py:210
  465.7 1.2 copy-start.5
  469.0 4.7 copy-start.8
  469.0 27.8 %all-to-all-start.1 = ((bf16[4,128,2048]{2,1,0:T(8,128)(2,1)}), bf16[4,128,2048]{2,1,0:T(8,128)(2,1)}, u32[]{:S(2)}, u32[]{:S(2)}) async-start(bf16[4,128,2048]{2,1,0:T(8,128)(2,1)} %bitcast.7), calls=%async_computation.1 | async-start | bytes 4194304 | tf_op jit(solution)/shard_map/all_to_all | solution.py:40
  477.3 21.9 %copy-start.7 = (f32[2048]{0:T(1024)S(1)}, f32[2048]{0:T(1024)}, u32[]{:S(2)}) copy-start(f32[2048]{0:T(1024)} %param.26) | copy-start | bytes 24580
  496.8 3.4 copy-start.1
Sparse Core Ops, SparseCore 0:
  115.2 69.5 all-gather.4
  187.3 101.4 all-gather.2
where the time goes:
time: 510 us; the launch traced here: 507 us
  blocking collectives  138 us (27%)
  local copies, waits for them, and re-layouts  99.6 us (20%)
  waiting for transfers between devices  96.2 us (19%)
  matrix products  95.2 us (19%)
  other arithmetic  36.6 us (7%)
  starting transfers between devices  23.3 us (5%)
  between operations  14.4 us (3%)
    all_to_all x1, blocking collectives, on_device(): lax.all_to_all(outgoing, 'ep', split_axis=0, concat_axis=0, tiled=True)  98.5 us
    all_to_all x2, waiting for transfers between devices, summed_on_arrival(): lax.all_to_all(parts, axis, split_axis=0, concat_axis=0, tiled=True)  70.6 us
    all_to_all x1, blocking collectives, sent_to_all(): return lax.all_to_all(copies, axis, split_axis=0, concat_axis=0, tiled=True)  39.8 us
    dynamic_slice x32, local copies, waits for them, and re-layouts, advance_increment(): lax.dynamic_slice_in_dim(value_part, offset, block_size, 0)  34.1 us
    dot_general x32, matrix products, compute(): jnp.einsum('hqk,khd->hqd', weights.astype(jnp.bfloat16), value_heads, pre...  29.3 us
    all_gather x1, waiting for transfers between devices, on_device(): lax.all_gather(arrived, 'tp', axis=0, tiled=True)  25.5 us
    dot_general x32, matrix products, compute(): jnp.einsum('qhd,khd->hqk', queries, key_heads, preferred_element_type=jnp...  24.7 us
    dynamic_slice x32, local copies, waits for them, and re-layouts, compute(): key_gate = lax.dynamic_slice_in_dim(forget_cumsum, key_first, key_count, 1)  22.2 us
  transfers between devices with their start and end apart: 5, of which 3 were waited for; matrix products, arithmetic and copies ran while one was open for 43% of the time, Pallas kernels for 0%

commit v1 on v0

v1 whole, which is shorter than its diff:
```python
import functools

import jax
import jax.numpy as jnp
from jax import lax
from jax.experimental import pallas as pl
from jax.experimental.pallas import tpu as pltpu
from jax.sharding import PartitionSpec as P

EPS = 1e-06
MASKED = -1e30
LOG2E = 1.4426950408889634
MESH = pl.DeviceIdType.MESH
SUB, LANE = 16, 128
BF16, F32 = jnp.bfloat16, jnp.float32
ANY = pl.BlockSpec(memory_space=pl.ANY)
VM = pl.BlockSpec(memory_space=pltpu.VMEM)


def normalize(row_block, gain):
    values = row_block.astype(F32)
    inverse = lax.rsqrt(jnp.mean(values * values, axis=-1, keepdims=True) + EPS)
    return values * inverse * gain


def dot(a, b):
    return jnp.dot(a, b, preferred_element_type=F32)


def swap_matrix():
    n = SUB * SUB
    i = lax.broadcasted_iota(jnp.int32, (n, n), 0)
    k = lax.broadcasted_iota(jnp.int32, (n, n), 1)
    hit = ((i // SUB) == (k % SUB)) & ((i % SUB) == (k // SUB))
    return jnp.where(hit, 1.0, 0.0).astype(BF16)


def to_wire(swap, rows):
    halves = [
        jnp.concatenate(
            [rows[SUB * a : SUB * (a + 1), LANE * s : LANE * (s + 1)] for s in range(SUB)], axis=0
        )
        for a in range(2)
    ]
    out = dot(swap, jnp.concatenate(halves, axis=1)).astype(BF16)
    return jnp.concatenate([out[:, :LANE], out[:, LANE:]], axis=0)


def from_wire(swap, tiles):
    n = SUB * SUB
    out = dot(swap, jnp.concatenate([tiles[:n], tiles[n:]], axis=1)).astype(BF16)
    halves = [
        jnp.concatenate(
            [out[SUB * s : SUB * (s + 1), LANE * a : LANE * (a + 1)] for s in range(SUB)], axis=1
        )
        for a in range(2)
    ]
    return jnp.concatenate(halves, axis=0)


def slot_columns(routes, capacity):
    rows, top = routes.shape
    experts = lax.broadcasted_iota(jnp.int32, (rows, LANE), 1)
    earlier = lax.broadcasted_iota(jnp.int32, (rows, rows), 1) < lax.broadcasted_iota(
        jnp.int32, (rows, rows), 0
    )
    earlier = jnp.where(earlier, 1.0, 0.0).astype(BF16)
    taken = jnp.zeros((1, LANE), F32)
    columns = []
    for k in range(top):
        member = jnp.where(experts == routes[:, k : k + 1], 1.0, 0.0)
        before = dot(earlier, member.astype(BF16)) + taken
        rank = jnp.sum(before * member, axis=1, keepdims=True)
        columns.append(routes[:, k : k + 1].astype(F32) * capacity + rank)
        taken = taken + jnp.sum(member, axis=0, keepdims=True)
    return columns


def chooser(column, width):
    ids = lax.broadcasted_iota(jnp.int32, (column.shape[0], width), 1).astype(F32)
    return jnp.where(ids == column, 1.0, 0.0)


def greet(axes):
    barrier = pltpu.get_barrier_semaphore()
    total = 0
    for axis in axes:
        n = lax.axis_size(axis)
        me = lax.axis_index(axis)

        @pl.loop(1, n)
        def _(s):
            pl.semaphore_signal(
                barrier, inc=1, device_id={axis: lax.rem(me + s, n)}, device_id_type=MESH
            )

        total += n - 1
    return lambda: pl.semaphore_wait(barrier, total)


def exchange(send, land, block, send_sem, recv_sem):
    n = lax.axis_size("ep")
    me = lax.axis_index("ep")

    def copy(s):
        to = lax.rem(me + s, n)
        return pltpu.make_async_remote_copy(
            src_ref=send.at[pl.ds(pl.multiple_of(to * block, block), block)],
            dst_ref=land.at[pl.ds(pl.multiple_of(me * block, block), block)],
            send_sem=send_sem.at[s],
            recv_sem=recv_sem.at[s],
            device_id={"ep": to},
            device_id_type=MESH,
        )

    def start():
        half = n // 2

        @pl.loop(1, half)
        def _(s):
            copy(s).start()
            copy(n - s).start()

        copy(half).start()

    def wait():
        @pl.loop(1, n)
        def _(s):
            copy(s).wait()

    return start, wait


def first_kernel(
    capacity,
    x_ref, gain_ref, wq_ref, wk_ref, wv_ref, y_ref, ygain_ref, routes_ref,
    q_ref, kv_ref, land_ref,
    normed, weights, picked, send, w_sem, xs_sem, xr_sem, zs_sem, zr_sem,
):
    rows, width = x_ref.shape
    head_width = wq_ref.shape[1]
    tp, t = lax.axis_size("tp"), lax.axis_index("tp")
    ep, e = lax.axis_size("ep"), lax.axis_index("ep")
    slots = picked.shape[0]
    block = capacity * SUB
    loads = [
        pltpu.make_async_copy(w, weights.at[i], w_sem.at[i])
        for i, w in enumerate((wq_ref, wk_ref, wv_ref))
    ]
    for load in loads:
        load.start()
    met = greet(("ep", "tp"))

    own = pl.ds(pl.multiple_of(t * rows, rows), rows)
    normed[own, :] = normalize(x_ref[...], gain_ref[...]).astype(BF16)
    columns = slot_columns(routes_ref[...], capacity)
    padded = -(-slots // LANE) * LANE
    choose = sum(chooser(c, padded) for c in columns)
    expert_rows = normalize(y_ref[...], ygain_ref[...]).astype(BF16)
    picked[...] = dot(jnp.transpose(choose)[:slots].astype(BF16), expert_rows).astype(BF16)
    swap = swap_matrix()
    for c in range(slots // 32):
        send[pl.ds(c * 512, 512), :] = to_wire(swap, picked[pl.ds(c * 32, 32), :])
    met()
    start, wait = exchange(send, land_ref, block, zs_sem, zr_sem)

    def spread(j):
        return pltpu.make_async_remote_copy(
            src_ref=normed.at[own],
            dst_ref=normed.at[own],
            send_sem=xs_sem.at[j],
            recv_sem=xr_sem.at[j],
            device_id={"tp": lax.rem(t + j, tp)},
            device_id_type=MESH,
        )

    start()
    for j in (1, tp - 1) + tuple(range(2, tp - 1)):
        spread(j).start()
    mine = pl.ds(pl.multiple_of(e * block, block), block)
    land_ref[mine, :] = send[mine, :]
    for load in loads:
        load.wait()
    for j in (0, 1, tp - 1) + tuple(range(2, tp - 1)):
        if j:
            spread(j).wait_recv()
        part = pl.ds(pl.multiple_of(lax.rem(t + tp - j, tp) * rows, rows), rows)
        block_rows = normed[part, :]
        q_ref[part, :] = dot(block_rows, weights[0]).astype(BF16)
        kv_ref[part, :head_width] = dot(block_rows, weights[1]).astype(BF16)
        kv_ref[part, head_width:] = dot(block_rows, weights[2]).astype(BF16)
    for j in range(1, tp):
        spread(j).wait_send()
    wait()


def second_kernel(
    pieces,
    land_ref, gate_ref, up_ref, down_ref,
    back_ref,
    gate, up, down, stack, sums, theirs, w_sem, xs_sem, xr_sem, ps_sem, pr_sem,
):
    tp, t = lax.axis_size("tp"), lax.axis_index("tp")
    slots = sums.shape[1]
    piece = slots // pieces
    loads = [
        pltpu.make_async_copy(w, v, w_sem.at[i])
        for i, (w, v) in enumerate(((gate_ref, gate), (up_ref, up), (down_ref, down)))
    ]
    for load in loads:
        load.start()
    met = greet(("tp",))
    swap = swap_matrix()
    order = (1, tp - 1) + tuple(range(2, tp - 1))

    def forth(j, c):
        return pltpu.make_async_remote_copy(
            src_ref=land_ref.at[pl.ds(c * piece * SUB, piece * SUB)],
            dst_ref=stack.at[j - 1, pl.ds(c * piece * SUB, piece * SUB)],
            send_sem=xs_sem.at[j - 1, c],
            recv_sem=xr_sem.at[j - 1, c],
            device_id={"tp": lax.rem(t + j, tp)},
            device_id_type=MESH,
        )

    def back(j, c):
        return pltpu.make_async_remote_copy(
            src_ref=sums.at[j, pl.ds(c * piece, piece)],
            dst_ref=theirs.at[j - 1, pl.ds(c * piece, piece)],
            send_sem=ps_sem.at[j - 1, c],
            recv_sem=pr_sem.at[j - 1, c],
            device_id={"tp": lax.rem(t + tp - j, tp)},
            device_id_type=MESH,
        )

    def expert(j, c):
        wire = land_ref if j == 0 else stack.at[j - 1]
        rows = jnp.concatenate(
            [
                from_wire(swap, wire[pl.ds((c * piece + 32 * i) * SUB, 32 * SUB), :])
                for i in range(piece // 32)
            ],
            axis=0,
        )
        gate_proj = dot(rows, gate[0])
        hidden = (gate_proj / (1.0 + jnp.exp(-gate_proj)) * dot(rows, up[0])).astype(BF16)
        sums[j, pl.ds(c * piece, piece), :] = dot(hidden, down[0]).astype(BF16)

    met()
    for c in range(pieces):
        for j in order:
            forth(j, c).start()
    for load in loads:
        load.wait()
    for c in range(pieces):
        expert(0, c)
    for c in range(pieces):
        for j in order:
            forth(j, c).wait_recv()
            expert(j, c)
            back(j, c).start()
    for c in range(pieces):
        for j in order:
            back(j, c).wait_recv()
        for i in range(piece // 32):
            here = pl.ds(c * piece + 32 * i, 32)
            total = sums[0, here, :].astype(F32)
            for j in range(1, tp):
                total = total + theirs[j - 1, here, :].astype(F32)
            back_ref[pl.ds((c * piece + 32 * i) * SUB, 32 * SUB), :] = to_wire(
                swap, total.astype(BF16)
            )
    for c in range(pieces):
        for j in order:
            forth(j, c).wait_send()
            back(j, c).wait_send()


def third_kernel(
    capacity,
    q_ref, all_ref, forget_ref, wo_ref, post_ref, back_ref, routes_ref, rweight_ref,
    mix_ref, out_ref,
    keys, running_max, running_sum, running_acc, attended, parts, theirs, returned, natural,
    k_sem, zs_sem, zr_sem, xs_sem, xr_sem,
):
    tp, t = lax.axis_size("tp"), lax.axis_index("tp")
    e = lax.axis_index("ep")
    span = q_ref.shape[0]
    rows, width = mix_ref.shape
    heads = forget_ref.shape[0]
    head_dim = q_ref.shape[1] // heads
    head_width = heads * head_dim
    slots = natural.shape[0]
    block = capacity * SUB
    scale = head_dim ** (-0.5) * LOG2E

    def load(j, slot):
        return pltpu.make_async_copy(
            all_ref.at[pl.ds(pl.multiple_of(j * span, span), span)], keys.at[slot], k_sem.at[slot]
        )

    load(0, 0).start()
    met = greet(("ep", "tp"))
    running_max[...] = jnp.full_like(running_max, MASKED)
    running_sum[...] = jnp.zeros_like(running_sum)
    running_acc[...] = jnp.zeros_like(running_acc)
    met()
    start, wait = exchange(back_ref, returned, block, zs_sem, zr_sem)
    start()
    mine = pl.ds(pl.multiple_of(e * block, block), block)
    returned[mine, :] = back_ref[mine, :]
    first = pl.multiple_of(e * span, span)
    base = forget_ref[:, pl.ds(first, LANE)][:, :1]

    def attend(j, slot, masked):
        bias = (base - forget_ref[:, pl.ds(pl.multiple_of(j * span, span), span)]) * LOG2E
        for h in range(heads):
            cols = slice(h * head_dim, (h + 1) * head_dim)
            vcols = slice(head_width + h * head_dim, head_width + (h + 1) * head_dim)
            scores = lax.dot_general(
                q_ref[:, cols], keys[slot, :, cols], (((1,), (1,)), ((), ())),
                preferred_element_type=F32,
            )
            scores = scores * scale + bias[h : h + 1, :]
            if masked:
                seen = lax.broadcasted_iota(jnp.int32, (span, span), 1) <= (
                    lax.broadcasted_iota(jnp.int32, (span, span), 0)
                )
                scores = jnp.where(seen, scores, MASKED)
            old = running_max[h]
            new = jnp.maximum(old, jnp.max(scores, axis=1, keepdims=True))
            weights = jnp.exp2(scores - jnp.tile(new, (1, span // LANE)))
            rescale = jnp.exp2(old - new)
            partial = weights[:, :LANE]
            for i in range(1, span // LANE):
                partial = partial + weights[:, i * LANE : (i + 1) * LANE]
            running_sum[h] = running_sum[h] * rescale + partial
            running_acc[h] = running_acc[h] * rescale + dot(weights.astype(BF16), keys[slot, :, vcols])
            running_max[h] = new

    @pl.loop(0, e)
    def _(j):
        slot = lax.rem(j, 2)
        load(j + 1, 1 - slot).start()
        load(j, slot).wait()
        attend(j, slot, False)

    last = lax.rem(e, 2)
    load(e, last).wait()
    attend(e, last, True)
    for h in range(heads):
        total = jnp.sum(running_sum[h], axis=1, keepdims=True)
        attended[:, h * head_dim : (h + 1) * head_dim] = (running_acc[h] / total).astype(BF16)

    def spread(j):
        return pltpu.make_async_remote_copy(
            src_ref=parts.at[j],
            dst_ref=theirs.at[j - 1],
            send_sem=xs_sem.at[j - 1],
            recv_sem=xr_sem.at[j - 1],
            device_id={"tp": lax.rem(t + j, tp)},
            device_id_type=MESH,
        )

    order = tuple(range(2, tp - 1)) + (1, tp - 1)
    for j in order + (0,):
        here = pl.ds(pl.multiple_of(lax.rem(t + j, tp) * rows, rows), rows)
        parts[j] = dot(attended[here, :], wo_ref[...]).astype(BF16)
        if j:
            spread(j).start()

    wait()
    swap = swap_matrix()
    for c in range(slots // 32):
        natural[pl.ds(c * 32, 32), :] = from_wire(swap, returned[pl.ds(c * 512, 512), :])
    columns = slot_columns(routes_ref[...], capacity)
    combined = jnp.zeros((rows, width), F32)
    for k, column in enumerate(columns):
        choose = chooser(column, slots).astype(BF16)
        combined = combined + rweight_ref[:, k : k + 1] * dot(choose, natural[...])
    out_ref[...] = combined.astype(BF16)

    total = parts[0].astype(F32)
    for j in range(1, tp):
        spread(j).wait_recv()
        total = total + theirs[j - 1].astype(F32)
    mix_ref[...] = normalize(total, post_ref[...]).astype(BF16)
    for j in range(1, tp):
        spread(j).wait_send()


def dma(*shape):
    return pltpu.SemaphoreType.DMA(shape)


def params(number):
    return pltpu.CompilerParams(
        collective_id=number, has_side_effects=True, vmem_limit_bytes=60 * 1024 * 1024
    )


def on_device(
    mixer_input, forget_cumsum, mixer_gain, query_weight, key_weight, value_weight, out_weight,
    post_gain, expert_input, expert_gain, routes, route_weight, expert_gate, expert_upward, expert_down,
):
    ep, tp = lax.axis_size("ep"), lax.axis_size("tp")
    rows, width = mixer_input.shape
    heads = forget_cumsum.shape[0]
    head_width = query_weight.shape[1]
    head_dim = head_width // heads
    span = rows * tp
    moe_rows, top = routes.shape
    experts = ep * expert_gate.shape[0]
    capacity = (moe_rows * top * 9 + 8 * experts - 1) // (8 * experts)
    slots = experts * capacity
    hidden = expert_gate.shape[2]
    wire = jax.ShapeDtypeStruct((slots * SUB, LANE), BF16)

    queries, pairs, arrived = pl.pallas_call(
        functools.partial(first_kernel, capacity),
        name="first",
        out_shape=(
            jax.ShapeDtypeStruct((span, head_width), BF16),
            jax.ShapeDtypeStruct((span, 2 * head_width), BF16),
            wire,
        ),
        in_specs=[VM, VM, ANY, ANY, ANY, VM, VM, VM],
        out_specs=(VM, VM, VM),
        scratch_shapes=[
            pltpu.VMEM((span, width), BF16),
            pltpu.VMEM((3, width, head_width), BF16),
            pltpu.VMEM((slots, width), BF16),
            pltpu.VMEM((slots * SUB, LANE), BF16),
            dma(3), dma(tp), dma(tp), dma(ep), dma(ep),
        ],
        compiler_params=params(0),
        cost_estimate=pl.CostEstimate(flops=4 * 10**9, bytes_accessed=10**8, transcendentals=0),
    )(
        mixer_input, mixer_gain[None], query_weight, key_weight, value_weight,
        expert_input, expert_gain[None], routes,
    )
    everyone = lax.all_gather(pairs, "ep", axis=0, tiled=True)

    pieces = 3
    back = pl.pallas_call(
        functools.partial(second_kernel, pieces),
        name="second",
        out_shape=wire,
        in_specs=[VM, ANY, ANY, ANY],
        out_specs=VM,
        scratch_shapes=[
            pltpu.VMEM((1, width, hidden), BF16),
            pltpu.VMEM((1, width, hidden), BF16),
            pltpu.VMEM((1, hidden, width), BF16),
            pltpu.VMEM((tp - 1, slots * SUB, LANE), BF16),
            pltpu.VMEM((tp, slots, width), BF16),
            pltpu.VMEM((tp - 1, slots, width), BF16),
            dma(3), dma(tp - 1, pieces), dma(tp - 1, pieces), dma(tp - 1, pieces), dma(tp - 1, pieces),
        ],
        compiler_params=params(1),
        cost_estimate=pl.CostEstimate(flops=8 * 10**9, bytes_accessed=2 * 10**8, transcendentals=0),
    )(arrived, expert_gate, expert_upward, expert_down)

    return pl.pallas_call(
        functools.partial(third_kernel, capacity),
        name="third",
        out_shape=(
            jax.ShapeDtypeStruct((rows, width), BF16),
            jax.ShapeDtypeStruct((moe_rows, width), BF16),
        ),
        in_specs=[VM, ANY, VM, VM, VM, VM, VM, VM],
        out_specs=(VM, VM),
        scratch_shapes=[
            pltpu.VMEM((2, span, 2 * head_width), BF16),
            pltpu.VMEM((heads, span, LANE), F32),
            pltpu.VMEM((heads, span, LANE), F32),
            pltpu.VMEM((heads, span, head_dim), F32),
            pltpu.VMEM((span, head_width), BF16),
            pltpu.VMEM((tp, rows, width), BF16),
            pltpu.VMEM((tp - 1, rows, width), BF16),
            pltpu.VMEM((slots * SUB, LANE), BF16),
            pltpu.VMEM((slots, width), BF16),
            dma(2), dma(ep), dma(ep), dma(tp - 1), dma(tp - 1),
        ],
        compiler_params=params(2),
        cost_estimate=pl.CostEstimate(flops=8 * 10**9, bytes_accessed=2 * 10**8, transcendentals=0),
    )(queries, everyone, forget_cumsum, out_weight, post_gain[None], back, routes, route_weight)


def solution(mesh):
    rows = P(("grp", "ep", "tp"), None)
    in_specs = (
        rows, P("tp", "grp"), P(), P(None, "tp"), P(None, "tp"), P(None, "tp"), P("tp", None), P(),
        rows, P(), rows, rows, P("ep", None, "tp"), P("ep", None, "tp"), P("ep", "tp", None),
    )
    return jax.shard_map(
        on_device, mesh=mesh, in_specs=in_specs, out_specs=(rows, rows), check_vma=False
    )
```

time: 510 us -> 281 us (0.55)
  the two profiles are of different devices: /device:TPU:1953 before, /device:TPU:33 now
where the time goes in v1:
time: 281 us; the launch traced here: 276 us
  Pallas kernels  252 us (90%)
  between operations  14.1 us (5%)
  local copies, waits for them, and re-layouts  5.92 us (2%)
  waiting for transfers between devices  3.45 us (1%)
    pallas_call x1, Pallas kernels, on_device(): pl.pallas_call(functools.partial(second_kernel, pieces), name='second', o...  103 us
    pallas_call x1, Pallas kernels, on_device(): pl.pallas_call(functools.partial(first_kernel, capacity), name='first', o...  78.4 us
    pallas_call x1, Pallas kernels, on_device(): pl.pallas_call(functools.partial(third_kernel, capacity), name='third', o...  70.5 us
    unnamed x6, local copies, waits for them, and re-layouts  5.92 us
  transfers between devices with their start and end apart: 1, of which 1 were waited for; matrix products, arithmetic and copies ran while one was open for 0% of the time, Pallas kernels for 37%

profile of v1, /device:TPU:33, one launch (start us, length us, event | category | flops | bytes accessed | tf_op | source)
XLA Modules:
  0.0 275.5 jit_solution(13524067350754522459)
XLA Ops:
  7.2 0.1 all-gather.2.cloned.1.call-start
  7.2 1.4 copy.17.routes_ref
  8.7 0.0 copy-start
  8.7 78.4 %first.1 = (bf16[512,256]{1,0:T(8,128)(2,1)}, bf16[512,512]{1,0:T(8,128)(2,1)}, bf16[4608,128]{1,0:T(8,128)(2,1)}) custom-call(bf16[128,2048]{1,0:T(8,128)(2,1)} %x_ref.1, f32[1,2048]{1,0:T(1,128)} %bitcast.3, bf16[2048,256]{1,0:T(8,128)(2,1)} %wq_ref.1, bf16[2048,256]{1,0:T(8,128)(2,1)} %wk_ref.1, bf16[2048,256]{1,0:T(8,128)(2,1)} %wv_ref.1, ...), custom_call_target="tpu_custom_call" | custom-call | flops 4000000000 | bytes 100000000 | tf_op jit(solution)/shard_map/first/pallas_call | solution.py:419
  87.0 0.1 all-gather.2.cloned.1.call-update
  87.1 0.0 copy-done
  87.1 0.7 copy.19.rweight_ref
  87.8 103.1 %second.1.back_ref = bf16[4608,128]{1,0:T(8,128)(2,1)} custom-call(bf16[4608,128]{1,0:T(8,128)(2,1)} %get-tuple-element.7.land_ref, bf16[1,2048,512]{2,1,0:T(8,128)(2,1)} %gate_ref.1, bf16[1,2048,512]{2,1,0:T(8,128)(2,1)} %up_ref.1, bf16[1,512,2048]{2,1,0:T(8,128)(2,1)} %down_ref.1), custom_call_target="tpu_custom_call" | custom-call | flops 8000000000 | bytes 200000000 | tf_op jit(solution)/shard_map/second/pallas_call | solution.py:445
  191.0 3.4 %all-gather.2.cloned.1.call-done.all_ref = bf16[16384,512]{1,0:T(8,128)(2,1)} async-done(((bf16[512,512]{1,0:T(8,128)(2,1)}), bf16[16384,512]{1,0:T(8,128)(2,1)}) %all-gather.2.cloned.1.call-update) | async-done | bytes 16777232 | tf_op jit(solution)/shard_map/all_gather | solution.py:442
  194.4 70.5 %third.1 = (bf16[128,2048]{1,0:T(8,128)(2,1)}, bf16[128,2048]{1,0:T(8,128)(2,1)}) custom-call(bf16[512,256]{1,0:T(8,128)(2,1)} %get-tuple-element.5.q_ref, bf16[16384,512]{1,0:T(8,128)(2,1)} %all-gather.2.cloned.1.call-done.all_ref, f32[2,16384]{1,0:T(2,128)} %forget_ref.1, bf16[256,2048]{1,0:T(8,128)(2,1)} %wo_ref.1, f32[1,2048]{1,0:T(1,128)} %bitcast.5, ...), custom_call_target="tpu_custom_call" | custom-call | flops 8000000000 | bytes 200000000 | tf_op jit(solution)/shard_map/third/pallas_call | solution.py:464
  264.9 1.9 copy.22
  266.8 1.9 copy.23
Async XLA Ops:
  7.2 187.2 %all-gather.2.cloned.1.call-start = ((), (), s32[]{:S(2)}) async-start(), calls=%async_computation | async-start | bytes 17301504 | tf_op jit(solution)/shard_map/all_gather | solution.py:442
  8.7 78.4 %copy-start = (f32[128,2]{0,1:T(2,128)S(1)}, f32[128,2]{0,1:T(2,128)}, u32[]{:S(2)}) copy-start(f32[128,2]{0,1:T(2,128)} %param.26) | copy-start | bytes 3076
Sparse Core Ops, SparseCore 0:
  87.2 107.1 all-gather.1

commit v2 on v1

v2 whole, which is shorter than its diff:
```python
import functools

import jax
import jax.numpy as jnp
from jax import lax
from jax.experimental import pallas as pl
from jax.experimental.pallas import tpu as pltpu
from jax.sharding import PartitionSpec as P

EPS = 1e-06
MASKED = -1e30
LOG2E = 1.4426950408889634
MESH = pl.DeviceIdType.MESH
SUB, LANE = 16, 128
BF16, F32 = jnp.bfloat16, jnp.float32
ANY = pl.BlockSpec(memory_space=pl.ANY)
VM = pl.BlockSpec(memory_space=pltpu.VMEM)


def normalize(row_block, gain):
    values = row_block.astype(F32)
    inverse = lax.rsqrt(jnp.mean(values * values, axis=-1, keepdims=True) + EPS)
    return values * inverse * gain


def dot(a, b):
    return jnp.dot(a, b, preferred_element_type=F32)


def swap_matrix():
    n = SUB * SUB
    i = lax.broadcasted_iota(jnp.int32, (n, n), 0)
    k = lax.broadcasted_iota(jnp.int32, (n, n), 1)
    hit = ((i // SUB) == (k % SUB)) & ((i % SUB) == (k // SUB))
    return jnp.where(hit, 1.0, 0.0).astype(BF16)


def to_wire(swap, rows):
    count = rows.shape[0] // SUB
    halves = [
        jnp.concatenate(
            [rows[SUB * a : SUB * (a + 1), LANE * s : LANE * (s + 1)] for s in range(SUB)], axis=0
        )
        for a in range(count)
    ]
    out = dot(swap, jnp.concatenate(halves, axis=1)).astype(BF16)
    return jnp.concatenate([out[:, LANE * a : LANE * (a + 1)] for a in range(count)], axis=0)


def from_wire(swap, tiles):
    n = SUB * SUB
    count = tiles.shape[0] // n
    out = dot(swap, jnp.concatenate([tiles[n * a : n * (a + 1)] for a in range(count)], axis=1))
    out = out.astype(BF16)
    halves = [
        jnp.concatenate(
            [out[SUB * s : SUB * (s + 1), LANE * a : LANE * (a + 1)] for s in range(SUB)], axis=1
        )
        for a in range(count)
    ]
    return jnp.concatenate(halves, axis=0)


def slot_columns(routes, capacity):
    rows, top = routes.shape
    experts = lax.broadcasted_iota(jnp.int32, (rows, LANE), 1)
    earlier = lax.broadcasted_iota(jnp.int32, (rows, rows), 1) < lax.broadcasted_iota(
        jnp.int32, (rows, rows), 0
    )
    earlier = jnp.where(earlier, 1.0, 0.0).astype(BF16)
    taken = jnp.zeros((1, LANE), F32)
    columns = []
    for k in range(top):
        member = jnp.where(experts == routes[:, k : k + 1], 1.0, 0.0)
        before = dot(earlier, member.astype(BF16)) + taken
        rank = jnp.sum(before * member, axis=1, keepdims=True)
        columns.append(routes[:, k : k + 1].astype(F32) * capacity + rank)
        taken = taken + jnp.sum(member, axis=0, keepdims=True)
    return columns


def chooser(column, width):
    ids = lax.broadcasted_iota(jnp.int32, (column.shape[0], width), 1).astype(F32)
    return jnp.where(ids == column, 1.0, 0.0)


def greet(axes):
    barrier = pltpu.get_barrier_semaphore()
    total = 0
    for axis in axes:
        n = lax.axis_size(axis)
        me = lax.axis_index(axis)

        @pl.loop(1, n)
        def _(s):
            pl.semaphore_signal(
                barrier, inc=1, device_id={axis: lax.rem(me + s, n)}, device_id_type=MESH
            )

        total += n - 1
    return lambda: pl.semaphore_wait(barrier, total)


def remote(src, dst, send_sem, recv_sem, **device):
    return pltpu.make_async_remote_copy(
        src_ref=src, dst_ref=dst, send_sem=send_sem, recv_sem=recv_sem,
        device_id=device, device_id_type=MESH,
    )


def aligned(start, size):
    return pl.ds(pl.multiple_of(start, size), size)


def kernel(
    capacity,
    x_ref, gain_ref, wq_ref, wk_ref, wv_ref, wo_ref, post_ref, forget_ref,
    y_ref, ygain_ref, routes_ref, rweight_ref, gate_ref, up_ref, down_ref,
    mix_ref, out_ref,
    normed, qkv_w, queries, keys, out_w, running_max, running_sum, running_acc, attended, parts, mix_theirs,
    natural, send, stack, gate, up, down, sums, theirs, back, returned,
    w_sem, ns_sem, nr_sem, zs_sem, zr_sem, gs_sem, gr_sem, ps_sem, pr_sem, bs_sem, br_sem, ms_sem, mr_sem,
    rs_sem, rr_sem, cs_sem, cr_sem,
):
    rows, width = x_ref.shape
    head_width = wq_ref.shape[1]
    heads = forget_ref.shape[0]
    head_dim = head_width // heads
    tp, t = lax.axis_size("tp"), lax.axis_index("tp")
    ep, e = lax.axis_size("ep"), lax.axis_index("ep")
    chips, chip, core = ep // 2, e // 2, lax.rem(e, 2)
    span = rows * tp
    slots = natural.shape[0]
    block = capacity * SUB
    pieces = 2
    piece = slots // pieces
    groups = 8
    group = ep // groups
    peers = (1, tp - 1) + tuple(range(2, tp - 1))

    loads = [
        pltpu.make_async_copy(src, dst, w_sem.at[i])
        for i, (src, dst) in enumerate(
            (
                (wq_ref, qkv_w.at[0]), (wk_ref, qkv_w.at[1]), (wv_ref, qkv_w.at[2]),
                (gate_ref, gate), (up_ref, up), (down_ref, down), (wo_ref, out_w),
            )
        )
    ]
    for load in loads:
        load.start()
    met = greet(("ep", "tp"))

    columns = slot_columns(routes_ref[...], capacity)
    padded = -(-slots // LANE) * LANE
    choose = sum(chooser(c, padded) for c in columns)
    expert_rows = normalize(y_ref[...], ygain_ref[...]).astype(BF16)
    natural[...] = dot(jnp.transpose(choose)[:slots].astype(BF16), expert_rows).astype(BF16)
    swap = swap_matrix()
    for c in range(slots // 32):
        send[pl.ds(c * 512, 512), :] = to_wire(swap, natural[pl.ds(c * 32, 32), :])
    met()

    def offset(p):
        return lax.rem(p, 2) * ((p + 1) // 2) + (1 - lax.rem(p, 2)) * (ep - p // 2)

    def dispatch(p):
        to = lax.rem(e + offset(p), ep)
        return remote(
            send.at[aligned(to * block, block)], stack.at[0, aligned(p * block, block)],
            zs_sem.at[p], zr_sem.at[p], ep=to,
        )

    @pl.loop(1, ep)
    def _(p):
        dispatch(p).start()

    stack[0, :block, :] = send[aligned(e * block, block), :]

    own = aligned(t * rows, rows)
    normed[own, :] = normalize(x_ref[...], gain_ref[...]).astype(BF16)

    def spread(j):
        return remote(
            normed.at[own], normed.at[own], ns_sem.at[j - 1], nr_sem.at[j - 1], tp=lax.rem(t + j, tp)
        )

    for j in peers:
        spread(j).start()
    running_max[...] = jnp.full_like(running_max, MASKED)
    running_sum[...] = jnp.zeros_like(running_sum)
    running_acc[...] = jnp.zeros_like(running_acc)
    for load in loads:
        load.wait()
    for j in (0,) + peers:
        if j:
            spread(j).wait_recv()
        part = aligned(lax.rem(t + tp - j, tp) * rows, rows)
        block_rows = normed[part, :]
        queries[part, :] = dot(block_rows, qkv_w[0]).astype(BF16)
        for half in range(2):
            keys[e, half, part, :] = dot(block_rows, qkv_w[1 + half]).astype(BF16)

    def source(way, h):
        return lax.rem(chip + (chips - h if way == 0 else h), chips)

    def hop(way, half, h):
        at = 2 * source(way, h - 1) + core
        to = lax.rem(e + (2 if way == 0 else ep - 2), ep)
        return remote(
            keys.at[at, half], keys.at[at, half], rs_sem.at[way, half, h], rr_sem.at[way, half, h], ep=to
        )

    def share(way, half, h):
        at = 2 * source(way, h) + core
        return remote(
            keys.at[at, half], keys.at[at, half], cs_sem.at[way, half, h], cr_sem.at[way, half, h],
            ep=e + 1 - 2 * core,
        )

    def farthest(way, half):
        return chips // 2 if way == half else chips // 2 - 1

    def comes(way, half, h):
        near = h <= farthest(way, half)
        return near & (chip >= h if way == 0 else lax.rem(chip + h, chips) < chips // 2)

    def needed(way, half, h):
        return (h <= farthest(way, half)) & (chip >= h if way == 0 else chip + h >= chips)

    def goes(way, half, h):
        near = h <= farthest(way, half)
        if way == 0:
            return near & (chip >= h - 1) & (chip + 1 < chips)
        return near & (lax.rem(chip + h - 1, chips) < chips // 2)

    WAYS = [(way, half) for half in range(2) for way in range(2)]
    for way, half in WAYS:
        @pl.when(goes(way, half, 1))
        def _():
            hop(way, half, 1).start()

    for half in range(2):
        share(0, half, 0).start()

    def forth(j, g):
        size = group * block
        return remote(
            stack.at[0, aligned(g * size, size)], stack.at[j, aligned(g * size, size)],
            gs_sem.at[j - 1, g], gr_sem.at[j - 1, g], tp=lax.rem(t + j, tp),
        )

    def back_to(j, p):
        return remote(
            sums.at[j, aligned(p * piece, piece)], theirs.at[j - 1, aligned(p * piece, piece)],
            ps_sem.at[j - 1, p], pr_sem.at[j - 1, p], tp=lax.rem(t + tp - j, tp),
        )

    def expert(j, p):
        tiles = piece * SUB
        half_tiles = 256 * (piece // SUB // 2)
        start = p * tiles
        got = [
            from_wire(swap, stack[j, pl.ds(pl.multiple_of(start + at, 256), size), :])
            for at, size in ((0, half_tiles), (half_tiles, tiles - half_tiles))
        ]
        batch = jnp.concatenate(got, axis=0)
        gate_proj = dot(batch, gate[0])
        hidden = (gate_proj / (1.0 + jnp.exp(-gate_proj)) * dot(batch, up[0])).astype(BF16)
        sums[j, aligned(p * piece, piece), :] = dot(hidden, down[0]).astype(BF16)

    @pl.loop(0, groups)
    def _(g):
        @pl.loop(0, group)
        def _(i):
            @pl.when(g * group + i > 0)
            def _():
                dispatch(g * group + i).wait_recv()

        for j in peers:
            forth(j, g).start()

    @pl.loop(0, pieces)
    def _(p):
        expert(0, p)

    def serve(p):
        @pl.loop(1, tp)
        def _(i):
            j = i + (i // 2) * (1 - 2 * lax.rem(i, 2))

            @pl.loop(0, groups // pieces)
            def _(g):
                forth(j, p * (groups // pieces) + g).wait_recv()

            expert(j, p)
            back_to(j, p).start()

    def give_back(p):
        from_here = lax.rem(e + ep - offset(p), ep)
        return remote(
            back.at[aligned(p * block, block)], returned.at[aligned(e * block, block)],
            bs_sem.at[p], br_sem.at[p], ep=from_here,
        )

    def reduce(p):
        for j in peers:
            back_to(j, p).wait_recv()

        @pl.loop(0, piece // SUB)
        def _(i):
            here = pl.ds(pl.multiple_of(p * piece + SUB * i, SUB), SUB)
            total = sums[0, here, :].astype(F32)
            for j in range(1, tp):
                total = total + theirs[j - 1, here, :].astype(F32)
            back[pl.ds(pl.multiple_of((p * piece + SUB * i) * SUB, 256), 256), :] = to_wire(
                swap, total.astype(BF16)
            )

        @pl.loop(0, ep // pieces)
        def _(i):
            @pl.when(p * (ep // pieces) + i > 0)
            def _():
                give_back(p * (ep // pieces) + i).start()

    scale = head_dim ** (-0.5) * LOG2E
    base = forget_ref[:, aligned(e * span, span)][:, :1]

    def attend(j, masked):
        bias = (base - forget_ref[:, aligned(j * span, span)]) * LOG2E
        for h in range(heads):
            cols = slice(h * head_dim, (h + 1) * head_dim)
            scores = lax.dot_general(
                queries[:, cols], keys[j, 0, :, cols], (((1,), (1,)), ((), ())),
                preferred_element_type=F32,
            )
            scores = scores * scale + bias[h : h + 1, :]
            if masked:
                seen = lax.broadcasted_iota(jnp.int32, (span, span), 1) <= (
                    lax.broadcasted_iota(jnp.int32, (span, span), 0)
                )
                scores = jnp.where(seen, scores, MASKED)
            old = running_max[h]
            new = jnp.maximum(old, jnp.max(scores, axis=1, keepdims=True))
            weights = jnp.exp2(scores - jnp.tile(new, (1, span // LANE)))
            rescale = jnp.exp2(old - new)
            partial = weights[:, :LANE]
            for i in range(1, span // LANE):
                partial = partial + weights[:, i * LANE : (i + 1) * LANE]
            running_sum[h] = running_sum[h] * rescale + partial
            running_acc[h] = running_acc[h] * rescale + dot(weights.astype(BF16), keys[j, 1, :, cols])
            running_max[h] = new

    attend(e, True)
    last = chips // 2

    @pl.loop(1, last + 2)
    def _(h):
        for way, half in WAYS:
            @pl.when(comes(way, half, h))
            def _():
                hop(way, half, h).wait_recv()

                @pl.when(goes(way, half, h + 1))
                def _():
                    hop(way, half, h + 1).start()

                @pl.when(needed(way, half, h))
                def _():
                    share(way, half, h).start()

        g = h - 1
        for way, half in WAYS:
            @pl.when(needed(way, half, g) if way == 0 else needed(way, half, g) & (g > 0))
            def _():
                share(way, half, g).wait_recv()

        @pl.loop(0, 4)
        def _(i):
            side, parity = i // 2, lax.rem(i, 2)
            away = (g > 0) & (
                ((side == 0) & (chip >= g)) | ((side == 1) & (chip + g >= chips) & (g < last))
            )
            home = (g == 0) & (i == 0) & (core == 1)

            @pl.when(away | home)
            def _():
                attend(2 * (chip - g + side * (2 * g - chips)) + parity, False)

        @pl.when((h == 2) | (h == 4))
        def _():
            serve(h // 2 - 1)

        @pl.when((h == 6) | (h == 8))
        def _():
            reduce(h // 2 - 3)

    for h in range(heads):
        total = jnp.sum(running_sum[h], axis=1, keepdims=True)
        attended[:, h * head_dim : (h + 1) * head_dim] = (running_acc[h] / total).astype(BF16)

    def mix_to(j):
        return remote(
            parts.at[j], mix_theirs.at[j - 1], ms_sem.at[j - 1], mr_sem.at[j - 1], tp=lax.rem(t + j, tp)
        )

    for j in tuple(range(2, tp - 1)) + (1, tp - 1, 0):
        here = aligned(lax.rem(t + j, tp) * rows, rows)
        parts[j] = dot(attended[here, :], out_w[...]).astype(BF16)
        if j:
            mix_to(j).start()

    returned[aligned(e * block, block), :] = back[:block, :]

    @pl.loop(1, ep)
    def _(p):
        give_back(p).wait_recv()

    for c in range(slots // 32):
        natural[pl.ds(c * 32, 32), :] = from_wire(swap, returned[pl.ds(c * 512, 512), :])
    columns = slot_columns(routes_ref[...], capacity)
    combined = jnp.zeros((rows, width), F32)
    for k, column in enumerate(columns):
        chosen = chooser(column, slots).astype(BF16)
        combined = combined + rweight_ref[:, k : k + 1] * dot(chosen, natural[...])
    out_ref[...] = combined.astype(BF16)

    total = parts[0].astype(F32)
    for j in range(1, tp):
        mix_to(j).wait_recv()
        total = total + mix_theirs[j - 1].astype(F32)
    mix_ref[...] = normalize(total, post_ref[...]).astype(BF16)

    for j in range(1, tp):
        spread(j).wait_send()
        mix_to(j).wait_send()
        for p in range(pieces):
            back_to(j, p).wait_send()

        @pl.loop(0, groups)
        def _(g):
            forth(j, g).wait_send()

    @pl.loop(1, ep)
    def _(p):
        dispatch(p).wait_send()
        give_back(p).wait_send()

    for half in range(2):
        share(0, half, 0).wait_send()

    @pl.loop(1, last + 1)
    def _(h):
        for way, half in WAYS:
            @pl.when(goes(way, half, h))
            def _():
                hop(way, half, h).wait_send()

            @pl.when(needed(way, half, h))
            def _():
                share(way, half, h).wait_send()


def dma(*shape):
    return pltpu.SemaphoreType.DMA(shape)


def on_device(
    mixer_input, forget_cumsum, mixer_gain, query_weight, key_weight, value_weight, out_weight,
    post_gain, expert_input, expert_gain, routes, route_weight, expert_gate, expert_upward, expert_down,
):
    ep, tp = lax.axis_size("ep"), lax.axis_size("tp")
    rows, width = mixer_input.shape
    heads = forget_cumsum.shape[0]
    head_width = query_weight.shape[1]
    head_dim = head_width // heads
    span = rows * tp
    moe_rows, top = routes.shape
    experts = ep * expert_gate.shape[0]
    capacity = (moe_rows * top * 9 + 8 * experts - 1) // (8 * experts)
    slots = experts * capacity
    hidden = expert_gate.shape[2]
    vmem = pltpu.VMEM
    hops = ep // 4 + 3

    return pl.pallas_call(
        functools.partial(kernel, capacity),
        name="block",
        out_shape=(
            jax.ShapeDtypeStruct((rows, width), BF16),
            jax.ShapeDtypeStruct((moe_rows, width), BF16),
        ),
        in_specs=[VM, VM, ANY, ANY, ANY, ANY, VM, VM, VM, VM, VM, VM, ANY, ANY, ANY],
        out_specs=(VM, VM),
        scratch_shapes=[
            vmem((span, width), BF16),
            vmem((3, width, head_width), BF16),
            vmem((span, head_width), BF16),
            vmem((ep, 2, span, head_width), BF16),
            vmem((head_width, width), BF16),
            vmem((heads, span, LANE), F32),
            vmem((heads, span, LANE), F32),
            vmem((heads, span, head_dim), F32),
            vmem((span, head_width), BF16),
            vmem((tp, rows, width), BF16),
            vmem((tp - 1, rows, width), BF16),
            vmem((slots, width), BF16),
            vmem((slots * SUB, LANE), BF16),
            vmem((tp, slots * SUB, LANE), BF16),
            vmem((1, width, hidden), BF16),
            vmem((1, width, hidden), BF16),
            vmem((1, hidden, width), BF16),
            vmem((tp, slots, width), BF16),
            vmem((tp - 1, slots, width), BF16),
            vmem((slots * SUB, LANE), BF16),
            vmem((slots * SUB, LANE), BF16),
            dma(7), dma(tp - 1), dma(tp - 1), dma(ep), dma(ep), dma(tp - 1, 8), dma(tp - 1, 8),
            dma(tp - 1, 2), dma(tp - 1, 2), dma(ep), dma(ep), dma(tp - 1), dma(tp - 1),
            dma(2, 2, hops), dma(2, 2, hops), dma(2, 2, hops), dma(2, 2, hops),
        ],
        compiler_params=pltpu.CompilerParams(
            collective_id=0, has_side_effects=True, vmem_limit_bytes=63 * 1024 * 1024
        ),
    )(
        mixer_input, mixer_gain[None], query_weight, key_weight, value_weight, out_weight,
        post_gain[None], forget_cumsum, expert_input, expert_gain[None], routes, route_weight,
        expert_gate, expert_upward, expert_down,
    )


def solution(mesh):
    rows = P(("grp", "ep", "tp"), None)
    in_specs = (
        rows, P("tp", "grp"), P(), P(None, "tp"), P(None, "tp"), P(None, "tp"), P("tp", None), P(),
        rows, P(), rows, rows, P("ep", None, "tp"), P("ep", None, "tp"), P("ep", "tp", None),
    )
    return jax.shard_map(
        on_device, mesh=mesh, in_specs=in_specs, out_specs=(rows, rows), check_vma=False
    )
```

time: 281 us -> 243 us (0.86); the launches traced: 276 us -> 243 us
  Pallas kernels: 252 us -> 235 us
  between operations: 14.1 us -> 0.64 us
  waiting for transfers between devices: 3.45 us -> 0 us
    pallas_call x3 -> x1, Pallas kernels: 252 us -> 235 us  [on_device(): pl.pallas_call(functools.partial(kernel, capacity), name='block', out_sha...]
    all_gather x1 -> x0, waiting for transfers between devices: 3.4 us -> none  [on_device(): everyone = lax.all_gather(pairs, 'ep', axis=0, tiled=True)]
    unnamed x6 -> x4, local copies, waits for them, and re-layouts: 5.92 us -> 6.59 us
  transfers between devices with their start and end apart: 1 -> 0, of which waited for: 1 -> 0; matrix products, arithmetic and copies ran while one was open for 0% -> 0% of each run, Pallas kernels for 37% -> 0%
where the time goes in v2:
time: 243 us
  Pallas kernels  235 us (97%)
  local copies, waits for them, and re-layouts  6.59 us (3%)
    pallas_call x1, Pallas kernels, on_device(): pl.pallas_call(functools.partial(kernel, capacity), name='block', out_sha...  235 us
    unnamed x4, local copies, waits for them, and re-layouts  6.59 us

profile of v2, /device:TPU:33, one launch (start us, length us, event | category | flops | bytes accessed | tf_op | source)
XLA Modules:
  0.0 242.6 jit_solution(16136586349114959431)
XLA Ops:
  0.6 1.4 copy.17.routes_ref
  2.0 1.4 copy.18.rweight_ref
  3.5 235.3 %block.1 = (bf16[128,2048]{1,0:T(8,128)(2,1)}, bf16[128,2048]{1,0:T(8,128)(2,1)}) custom-call(bf16[128,2048]{1,0:T(8,128)(2,1)} %x_ref.1, f32[1,2048]{1,0:T(1,128)} %bitcast.3, bf16[2048,256]{1,0:T(8,128)(2,1)} %wq_ref.1, bf16[2048,256]{1,0:T(8,128)(2,1)} %wk_ref.1, bf16[2048,256]{1,0:T(8,128)(2,1)} %wv_ref.1, bf16[256,2048]{1,0:T(8,128)(2,1)} %wo_ref.1, ...), custom_call_target="tpu_custom_call" | custom-call | tf_op jit(solution)/shard_map/block/pallas_call | solution.py:486
  238.8 1.9 copy.21
  240.7 1.9 copy.22

commit v3 on v2

--- a/solution.py
+++ b/solution.py
@@ -12,6 +12,9 @@
 LOG2E = 1.4426950408889634
 MESH = pl.DeviceIdType.MESH
 SUB, LANE = 16, 128
+TOP = 2
+SERVE = ((0, 0), (1, 5))
+REDUCE = ((0, 9), (1, 13))
 BF16, F32 = jnp.bfloat16, jnp.float32
 ANY = pl.BlockSpec(memory_space=pl.ANY)
 VM = pl.BlockSpec(memory_space=pltpu.VMEM)
@@ -61,9 +64,16 @@
     return jnp.concatenate(halves, axis=0)
 
 
+def upright(ref):
+    top, rows = ref.shape
+    return jnp.transpose(
+        jnp.concatenate([ref[...].astype(F32), jnp.zeros((8 - top, rows), F32)], axis=0)
+    )
+
+
 def slot_columns(routes, capacity):
-    rows, top = routes.shape
-    experts = lax.broadcasted_iota(jnp.int32, (rows, LANE), 1)
+    rows, top = routes.shape[0], TOP
+    experts = lax.broadcasted_iota(jnp.int32, (rows, LANE), 1).astype(F32)
     earlier = lax.broadcasted_iota(jnp.int32, (rows, rows), 1) < lax.broadcasted_iota(
         jnp.int32, (rows, rows), 0
     )
@@ -74,7 +84,7 @@
         member = jnp.where(experts == routes[:, k : k + 1], 1.0, 0.0)
         before = dot(earlier, member.astype(BF16)) + taken
         rank = jnp.sum(before * member, axis=1, keepdims=True)
-        columns.append(routes[:, k : k + 1].astype(F32) * capacity + rank)
+        columns.append(routes[:, k : k + 1] * capacity + rank)
         taken = taken + jnp.sum(member, axis=0, keepdims=True)
     return columns
 
@@ -110,6 +120,45 @@
 
 def aligned(start, size):
     return pl.ds(pl.multiple_of(start, size), size)
+
+
+def attend_block(queries, pair, bias, running_max, running_sum, running_acc, masked):
+    heads, span, head_dim = running_acc.shape
+    scale = head_dim ** (-0.5) * LOG2E
+    for h in range(heads):
+        cols = slice(h * head_dim, (h + 1) * head_dim)
+        scores = lax.dot_general(
+            queries[:, cols], pair[0, :, cols], (((1,), (1,)), ((), ())), preferred_element_type=F32
+        )
+        scores = scores * scale + bias[h : h + 1, :]
+        if masked:
+            seen = lax.broadcasted_iota(jnp.int32, (span, span), 1) <= (
+                lax.broadcasted_iota(jnp.int32, (span, span), 0)
+            )
+            scores = jnp.where(seen, scores, MASKED)
+        old = running_max[h]
+        new = jnp.maximum(old, jnp.max(scores, axis=1, keepdims=True))
+        weights = jnp.exp2(scores - jnp.tile(new, (1, span // LANE)))
+        rescale = jnp.exp2(old - new)
+        partial = weights[:, :LANE]
+        for i in range(1, span // LANE):
+            partial = partial + weights[:, i * LANE : (i + 1) * LANE]
+        running_sum[h] = running_sum[h] * rescale + partial
+        running_acc[h] = running_acc[h] * rescale + dot(weights.astype(BF16), pair[1, :, cols])
+        running_max[h] = new
+
+
+def expert_block(swap, stack, gate, up, down, sums, start, piece):
+    tiles = piece * SUB
+    half_tiles = 256 * (piece // SUB // 2)
+    got = [
+        from_wire(swap, stack[pl.ds(pl.multiple_of(start * SUB + at, 256), size), :])
+        for at, size in ((0, half_tiles), (half_tiles, tiles - half_tiles))
+    ]
+    batch = jnp.concatenate(got, axis=0)
+    gate_proj = dot(batch, gate[0])
+    hidden = (gate_proj / (1.0 + jnp.exp(-gate_proj)) * dot(batch, up[0])).astype(BF16)
+    sums[aligned(start, piece), :] = dot(hidden, down[0]).astype(BF16)
 
 
 def kernel(
@@ -151,7 +200,7 @@
         load.start()
     met = greet(("ep", "tp"))
 
-    columns = slot_columns(routes_ref[...], capacity)
+    columns = slot_columns(upright(routes_ref), capacity)
     padded = -(-slots // LANE) * LANE
     choose = sum(chooser(c, padded) for c in columns)
     expert_rows = normalize(y_ref[...], ygain_ref[...]).astype(BF16)
@@ -257,17 +306,7 @@
         )
 
     def expert(j, p):
-        tiles = piece * SUB
-        half_tiles = 256 * (piece // SUB // 2)
-        start = p * tiles
-        got = [
-            from_wire(swap, stack[j, pl.ds(pl.multiple_of(start + at, 256), size), :])
-            for at, size in ((0, half_tiles), (half_tiles, tiles - half_tiles))
-        ]
-        batch = jnp.concatenate(got, axis=0)
-        gate_proj = dot(batch, gate[0])
-        hidden = (gate_proj / (1.0 + jnp.exp(-gate_proj)) * dot(batch, up[0])).astype(BF16)
-        sums[j, aligned(p * piece, piece), :] = dot(hidden, down[0]).astype(BF16)
+        expert_block(swap, stack.at[j], gate, up, down, sums.at[j], p * piece, piece)
 
     @pl.loop(0, groups)
     def _(g):
@@ -284,17 +323,15 @@
     def _(p):
         expert(0, p)
 
-    def serve(p):
-        @pl.loop(1, tp)
-        def _(i):
-            j = i + (i // 2) * (1 - 2 * lax.rem(i, 2))
-
-            @pl.loop(0, groups // pieces)
-            def _(g):
-                forth(j, p * (groups // pieces) + g).wait_recv()
-
-            expert(j, p)
-            back_to(j, p).start()
+    def serve(i, p):
+        j = i + (i // 2) * (1 - 2 * (i % 2))
+
+        @pl.loop(0, groups // pieces)
+        def _(g):
+            forth(j, p * (groups // pieces) + g).wait_recv()
+
+        expert(j, p)
+        back_to(j, p).start()
 
     def give_back(p):
         from_here = lax.rem(e + ep - offset(p), ep)
@@ -323,40 +360,19 @@
             def _():
                 give_back(p * (ep // pieces) + i).start()
 
-    scale = head_dim ** (-0.5) * LOG2E
     base = forget_ref[:, aligned(e * span, span)][:, :1]
 
     def attend(j, masked):
         bias = (base - forget_ref[:, aligned(j * span, span)]) * LOG2E
-        for h in range(heads):
-            cols = slice(h * head_dim, (h + 1) * head_dim)
-            scores = lax.dot_general(
-                queries[:, cols], keys[j, 0, :, cols], (((1,), (1,)), ((), ())),
-                preferred_element_type=F32,
-            )
-            scores = scores * scale + bias[h : h + 1, :]
-            if masked:
-                seen = lax.broadcasted_iota(jnp.int32, (span, span), 1) <= (
-                    lax.broadcasted_iota(jnp.int32, (span, span), 0)
-                )
-                scores = jnp.where(seen, scores, MASKED)
-            old = running_max[h]
-            new = jnp.maximum(old, jnp.max(scores, axis=1, keepdims=True))
-            weights = jnp.exp2(scores - jnp.tile(new, (1, span // LANE)))
-            rescale = jnp.exp2(old - new)
-            partial = weights[:, :LANE]
-            for i in range(1, span // LANE):
-                partial = partial + weights[:, i * LANE : (i + 1) * LANE]
-            running_sum[h] = running_sum[h] * rescale + partial
-            running_acc[h] = running_acc[h] * rescale + dot(weights.astype(BF16), keys[j, 1, :, cols])
-            running_max[h] = new
+        attend_block(
+            queries, keys.at[j], bias, running_max, running_sum, running_acc, masked
+        )
 
     attend(e, True)
     last = chips // 2
 
-    @pl.loop(1, last + 2)
-    def _(h):
-        for way, half in WAYS:
+    def pump(half, h):
+        for way in range(2):
             @pl.when(comes(way, half, h))
             def _():
                 hop(way, half, h).wait_recv()
@@ -369,31 +385,43 @@
                 def _():
                     share(way, half, h).start()
 
+    @pl.loop(0, 2 * last + 2)
+    def _(u):
+        h, half = u // 2 + 1, lax.rem(u, 2)
         g = h - 1
-        for way, half in WAYS:
-            @pl.when(needed(way, half, g) if way == 0 else needed(way, half, g) & (g > 0))
-            def _():
-                share(way, half, g).wait_recv()
-
-        @pl.loop(0, 4)
-        def _(i):
-            side, parity = i // 2, lax.rem(i, 2)
+        for which in range(2):
+            @pl.when(half == which)
+            def _():
+                pump(which, h)
+
+        @pl.when(half == 0)
+        def _():
+            for way, what in WAYS:
+                @pl.when(needed(way, what, g))
+                def _():
+                    share(way, what, g).wait_recv()
+
+        @pl.loop(0, 2)
+        def _(parity):
             away = (g > 0) & (
-                ((side == 0) & (chip >= g)) | ((side == 1) & (chip + g >= chips) & (g < last))
+                ((half == 0) & (chip >= g)) | ((half == 1) & (chip + g >= chips) & (g < last))
             )
-            home = (g == 0) & (i == 0) & (core == 1)
+            home = (u == 0) & (parity == 0) & (core == 1)
 
             @pl.when(away | home)
             def _():
-                attend(2 * (chip - g + side * (2 * g - chips)) + parity, False)
-
-        @pl.when((h == 2) | (h == 4))
-        def _():
-            serve(h // 2 - 1)
-
-        @pl.when((h == 6) | (h == 8))
-        def _():
-            reduce(h // 2 - 3)
+                attend(2 * (chip - g + half * (2 * g - chips)) + parity, False)
+
+        for p, first in SERVE:
+            for i in range(1, tp):
+                @pl.when(u == first + i - 1)
+                def _():
+                    serve(i, p)
+
+        for p, at in REDUCE:
+            @pl.when(u == at)
+            def _():
+                reduce(p)
 
     for h in range(heads):
         total = jnp.sum(running_sum[h], axis=1, keepdims=True)
@@ -418,11 +446,12 @@
 
     for c in range(slots // 32):
         natural[pl.ds(c * 32, 32), :] = from_wire(swap, returned[pl.ds(c * 512, 512), :])
-    columns = slot_columns(routes_ref[...], capacity)
+    columns = slot_columns(upright(routes_ref), capacity)
     combined = jnp.zeros((rows, width), F32)
+    rweight = upright(rweight_ref)
     for k, column in enumerate(columns):
         chosen = chooser(column, slots).astype(BF16)
-        combined = combined + rweight_ref[:, k : k + 1] * dot(chosen, natural[...])
+        combined = combined + rweight[:, k : k + 1] * dot(chosen, natural[...])
     out_ref[...] = combined.astype(BF16)
 
     total = parts[0].astype(F32)
@@ -459,6 +488,11 @@
             @pl.when(needed(way, half, h))
             def _():
                 share(way, half, h).wait_send()
+
+
+def hand_over(mix_ref, out_ref, mix_result, out_result):
+    mix_result[...] = mix_ref[...]
+    out_result[...] = out_ref[...]
 
 
 def dma(*shape):
@@ -483,7 +517,7 @@
     vmem = pltpu.VMEM
     hops = ep // 4 + 3
 
-    return pl.pallas_call(
+    results = pl.pallas_call(
         functools.partial(kernel, capacity),
         name="block",
         out_shape=(
@@ -523,9 +557,16 @@
         ),
     )(
         mixer_input, mixer_gain[None], query_weight, key_weight, value_weight, out_weight,
-        post_gain[None], forget_cumsum, expert_input, expert_gain[None], routes, route_weight,
+        post_gain[None], forget_cumsum, expert_input, expert_gain[None], routes.T, route_weight.T,
         expert_gate, expert_upward, expert_down,
     )
+    return pl.pallas_call(
+        hand_over,
+        name="hand_over",
+        out_shape=[jax.ShapeDtypeStruct(r.shape, r.dtype) for r in results],
+        in_specs=[VM, VM],
+        out_specs=[VM, VM],
+    )(*results)
 
 
 def solution(mesh):

time: 243 us -> 236 us (0.971)
  local copies, waits for them, and re-layouts: 6.59 us -> 0 us
    unnamed x4 -> x0, local copies, waits for them, and re-layouts: 6.59 us -> none
    pallas_call x1, Pallas kernels: 235 us -> 232 us  [on_device(): pl.pallas_call(functools.partial(kernel, capacity), name='block', out_sha...]
where the time goes in v3:
time: 236 us; the launch traced here: 235 us
  Pallas kernels  234 us (99%)
    pallas_call x1, Pallas kernels, on_device(): pl.pallas_call(functools.partial(kernel, capacity), name='block', out_sha...  232 us

profile of v3, /device:TPU:33, one launch (start us, length us, event | category | flops | bytes accessed | tf_op | source)
XLA Modules:
  0.0 234.6 jit_solution(7423456646821055957)
XLA Ops:
  0.6 231.7 %block.1 = (bf16[128,2048]{1,0:T(8,128)(2,1)}, bf16[128,2048]{1,0:T(8,128)(2,1)}) custom-call(bf16[128,2048]{1,0:T(8,128)(2,1)} %x_ref.1, f32[1,2048]{1,0:T(1,128)} %bitcast.5, bf16[2048,256]{1,0:T(8,128)(2,1)} %wq_ref.1, bf16[2048,256]{1,0:T(8,128)(2,1)} %wk_ref.1, bf16[2048,256]{1,0:T(8,128)(2,1)} %wv_ref.1, bf16[256,2048]{1,0:T(8,128)(2,1)} %wo_ref.1, ...), custom_call_target="tpu_custom_call" | custom-call | tf_op jit(solution)/shard_map/block/pallas_call | solution.py:520
  232.4 2.2 hand_over.1

commit v4 on v3

--- a/solution.py
+++ b/solution.py
@@ -15,6 +15,7 @@
 TOP = 2
 SERVE = ((0, 0), (1, 5))
 REDUCE = ((0, 9), (1, 13))
+GIVE = ((0, 32, 13),)
 BF16, F32 = jnp.bfloat16, jnp.float32
 ANY = pl.BlockSpec(memory_space=pl.ANY)
 VM = pl.BlockSpec(memory_space=pltpu.VMEM)
@@ -71,7 +72,7 @@
     )
 
 
-def slot_columns(routes, capacity):
+def slot_columns(routes):
     rows, top = routes.shape[0], TOP
     experts = lax.broadcasted_iota(jnp.int32, (rows, LANE), 1).astype(F32)
     earlier = lax.broadcasted_iota(jnp.int32, (rows, rows), 1) < lax.broadcasted_iota(
@@ -84,7 +85,7 @@
         member = jnp.where(experts == routes[:, k : k + 1], 1.0, 0.0)
         before = dot(earlier, member.astype(BF16)) + taken
         rank = jnp.sum(before * member, axis=1, keepdims=True)
-        columns.append(routes[:, k : k + 1] * capacity + rank)
+        columns.append((routes[:, k : k + 1], rank))
         taken = taken + jnp.sum(member, axis=0, keepdims=True)
     return columns
 
@@ -167,7 +168,7 @@
     y_ref, ygain_ref, routes_ref, rweight_ref, gate_ref, up_ref, down_ref,
     mix_ref, out_ref,
     normed, qkv_w, queries, keys, out_w, running_max, running_sum, running_acc, attended, parts, mix_theirs,
-    natural, send, stack, gate, up, down, sums, theirs, back, returned,
+    natural, send, stack, gate, up, down, sums, theirs, back, returned, picks, combined,
     w_sem, ns_sem, nr_sem, zs_sem, zr_sem, gs_sem, gr_sem, ps_sem, pr_sem, bs_sem, br_sem, ms_sem, mr_sem,
     rs_sem, rr_sem, cs_sem, cr_sem,
 ):
@@ -200,7 +201,7 @@
         load.start()
     met = greet(("ep", "tp"))
 
-    columns = slot_columns(upright(routes_ref), capacity)
+    columns = [expert * capacity + rank for expert, rank in slot_columns(upright(routes_ref))]
     padded = -(-slots // LANE) * LANE
     choose = sum(chooser(c, padded) for c in columns)
     expert_rows = normalize(y_ref[...], ygain_ref[...]).astype(BF16)
@@ -336,7 +337,7 @@
     def give_back(p):
         from_here = lax.rem(e + ep - offset(p), ep)
         return remote(
-            back.at[aligned(p * block, block)], returned.at[aligned(e * block, block)],
+            back.at[aligned(p * block, block)], returned.at[aligned(p * block, block)],
             bs_sem.at[p], br_sem.at[p], ep=from_here,
         )
 
@@ -354,11 +355,10 @@
                 swap, total.astype(BF16)
             )
 
-        @pl.loop(0, ep // pieces)
-        def _(i):
-            @pl.when(p * (ep // pieces) + i > 0)
-            def _():
-                give_back(p * (ep // pieces) + i).start()
+    def give(low, high):
+        @pl.loop(max(low, 1), high)
+        def _(p):
+            give_back(p).start()
 
     base = forget_ref[:, aligned(e * span, span)][:, :1]
 
@@ -423,6 +423,11 @@
             def _():
                 reduce(p)
 
+        for low, high, at in GIVE:
+            @pl.when(u == at)
+            def _():
+                give(low, high)
+
     for h in range(heads):
         total = jnp.sum(running_sum[h], axis=1, keepdims=True)
         attended[:, h * head_dim : (h + 1) * head_dim] = (running_acc[h] / total).astype(BF16)
@@ -438,27 +443,42 @@
         if j:
             mix_to(j).start()
 
-    returned[aligned(e * block, block), :] = back[:block, :]
-
-    @pl.loop(1, ep)
-    def _(p):
-        give_back(p).wait_recv()
-
-    for c in range(slots // 32):
-        natural[pl.ds(c * 32, 32), :] = from_wire(swap, returned[pl.ds(c * 512, 512), :])
-    columns = slot_columns(upright(routes_ref), capacity)
-    combined = jnp.zeros((rows, width), F32)
+    returned[:block, :] = back[:block, :]
+    half_slots = slots // 2
     rweight = upright(rweight_ref)
-    for k, column in enumerate(columns):
-        chosen = chooser(column, slots).astype(BF16)
-        combined = combined + rweight[:, k : k + 1] * dot(chosen, natural[...])
-    out_ref[...] = combined.astype(BF16)
+    places = []
+    for chosen_expert, rank in slot_columns(upright(routes_ref)):
+        ahead = chosen_expert - e.astype(F32)
+        ahead = jnp.where(ahead < 0, ahead + ep, ahead)
+        place = jnp.where(ahead > ep // 2, 2 * (ep - ahead), jnp.maximum(2 * ahead - 1, 0))
+        places.append(place * capacity + rank)
+    for stage in range(2):
+        picks[stage] = jnp.concatenate(
+            [chooser(place - stage * half_slots, half_slots) for place in places], axis=0
+        ).astype(BF16)
 
     total = parts[0].astype(F32)
     for j in range(1, tp):
         mix_to(j).wait_recv()
         total = total + mix_theirs[j - 1].astype(F32)
     mix_ref[...] = normalize(total, post_ref[...]).astype(BF16)
+
+    for stage in range(2):
+        @pl.loop(max(stage * (ep // 2), 1), (stage + 1) * (ep // 2))
+        def _(p):
+            give_back(p).wait_recv()
+
+        here = stage * half_slots
+        for at in range(0, half_slots, 48):
+            natural[pl.ds(here + at, 48), :] = from_wire(
+                swap, returned[pl.ds((here + at) * SUB, 48 * SUB), :]
+            )
+        both = dot(picks[stage], natural[pl.ds(here, half_slots), :])
+        result = rweight[:, :1] * both[:rows] + rweight[:, 1:2] * both[rows:]
+        if stage == 0:
+            combined[...] = result
+        else:
+            out_ref[...] = (combined[...] + result).astype(BF16)
 
     for j in range(1, tp):
         spread(j).wait_send()
@@ -548,6 +568,8 @@
             vmem((tp - 1, slots, width), BF16),
             vmem((slots * SUB, LANE), BF16),
             vmem((slots * SUB, LANE), BF16),
+            vmem((2, top * moe_rows, slots // 2), BF16),
+            vmem((moe_rows, width), F32),
             dma(7), dma(tp - 1), dma(tp - 1), dma(ep), dma(ep), dma(tp - 1, 8), dma(tp - 1, 8),
             dma(tp - 1, 2), dma(tp - 1, 2), dma(ep), dma(ep), dma(tp - 1), dma(tp - 1),
             dma(2, 2, hops), dma(2, 2, hops), dma(2, 2, hops), dma(2, 2, hops),

time: 236 us -> 225 us (0.953)
  the two profiles are of different devices: /device:TPU:33 before, /device:TPU:160 now
where the time goes in v4:
time: 225 us
  Pallas kernels  225 us (100%)
    pallas_call x1, Pallas kernels, on_device(): pl.pallas_call(functools.partial(kernel, capacity), name='block', out_sha...  222 us

profile of v4, /device:TPU:160, one launch (start us, length us, event | category | flops | bytes accessed | tf_op | source)
XLA Modules:
  0.0 225.2 jit_solution(9123070598429638231)
XLA Ops:
  0.6 222.4 %block.1 = (bf16[128,2048]{1,0:T(8,128)(2,1)}, bf16[128,2048]{1,0:T(8,128)(2,1)}) custom-call(bf16[128,2048]{1,0:T(8,128)(2,1)} %x_ref.1, f32[1,2048]{1,0:T(1,128)} %bitcast.5, bf16[2048,256]{1,0:T(8,128)(2,1)} %wq_ref.1, bf16[2048,256]{1,0:T(8,128)(2,1)} %wk_ref.1, bf16[2048,256]{1,0:T(8,128)(2,1)} %wv_ref.1, bf16[256,2048]{1,0:T(8,128)(2,1)} %wo_ref.1, ...), custom_call_target="tpu_custom_call" | custom-call | tf_op jit(solution)/shard_map/block/pallas_call | solution.py:540
  223.0 2.2 hand_over.1

commit v5 on v4

--- a/solution.py
+++ b/solution.py
@@ -15,7 +15,7 @@
 TOP = 2
 SERVE = ((0, 0), (1, 5))
 REDUCE = ((0, 9), (1, 13))
-GIVE = ((0, 32, 13),)
+NEAR, LOW = 13, 6
 BF16, F32 = jnp.bfloat16, jnp.float32
 ANY = pl.BlockSpec(memory_space=pl.ANY)
 VM = pl.BlockSpec(memory_space=pltpu.VMEM)
@@ -355,10 +355,19 @@
                 swap, total.astype(BF16)
             )
 
-    def give(low, high):
-        @pl.loop(max(low, 1), high)
+    def give():
+        @pl.loop(1, NEAR)
         def _(p):
             give_back(p).start()
+
+        for low in (True, False):
+            @pl.loop(NEAR, ep)
+            def _(p):
+                to_low = lax.rem(e + ep - offset(p), ep) < LOW
+
+                @pl.when(to_low if low else jnp.logical_not(to_low))
+                def _():
+                    give_back(p).start()
 
     base = forget_ref[:, aligned(e * span, span)][:, :1]
 
@@ -423,10 +432,9 @@
             def _():
                 reduce(p)
 
-        for low, high, at in GIVE:
-            @pl.when(u == at)
-            def _():
-                give(low, high)
+        @pl.when(u == REDUCE[-1][1])
+        def _():
+            give()
 
     for h in range(heads):
         total = jnp.sum(running_sum[h], axis=1, keepdims=True)
@@ -444,7 +452,7 @@
             mix_to(j).start()
 
     returned[:block, :] = back[:block, :]
-    half_slots = slots // 2
+    stages, batch = picks.shape[0], picks.shape[2]
     rweight = upright(rweight_ref)
     places = []
     for chosen_expert, rank in slot_columns(upright(routes_ref)):
@@ -452,37 +460,13 @@
         ahead = jnp.where(ahead < 0, ahead + ep, ahead)
         place = jnp.where(ahead > ep // 2, 2 * (ep - ahead), jnp.maximum(2 * ahead - 1, 0))
         places.append(place * capacity + rank)
-    for stage in range(2):
+    for stage in range(stages):
         picks[stage] = jnp.concatenate(
-            [chooser(place - stage * half_slots, half_slots) for place in places], axis=0
+            [chooser(place - stage * batch, batch) for place in places], axis=0
         ).astype(BF16)
-
-    total = parts[0].astype(F32)
-    for j in range(1, tp):
-        mix_to(j).wait_recv()
-        total = total + mix_theirs[j - 1].astype(F32)
-    mix_ref[...] = normalize(total, post_ref[...]).astype(BF16)
-
-    for stage in range(2):
-        @pl.loop(max(stage * (ep // 2), 1), (stage + 1) * (ep // 2))
-        def _(p):
-            give_back(p).wait_recv()
-
-        here = stage * half_slots
-        for at in range(0, half_slots, 48):
-            natural[pl.ds(here + at, 48), :] = from_wire(
-                swap, returned[pl.ds((here + at) * SUB, 48 * SUB), :]
-            )
-        both = dot(picks[stage], natural[pl.ds(here, half_slots), :])
-        result = rweight[:, :1] * both[:rows] + rweight[:, 1:2] * both[rows:]
-        if stage == 0:
-            combined[...] = result
-        else:
-            out_ref[...] = (combined[...] + result).astype(BF16)
 
     for j in range(1, tp):
         spread(j).wait_send()
-        mix_to(j).wait_send()
         for p in range(pieces):
             back_to(j, p).wait_send()
 
@@ -493,7 +477,6 @@
     @pl.loop(1, ep)
     def _(p):
         dispatch(p).wait_send()
-        give_back(p).wait_send()
 
     for half in range(2):
         share(0, half, 0).wait_send()
@@ -508,6 +491,33 @@
             @pl.when(needed(way, half, h))
             def _():
                 share(way, half, h).wait_send()
+
+    total = parts[0].astype(F32)
+    for j in range(1, tp):
+        mix_to(j).wait_recv()
+        total = total + mix_theirs[j - 1].astype(F32)
+    mix_ref[...] = normalize(total, post_ref[...]).astype(BF16)
+    for j in range(1, tp):
+        mix_to(j).wait_send()
+
+    for stage in range(stages):
+        here = stage * batch
+
+        @pl.loop(max(-(-here // capacity), 1), -(-(here + batch) // capacity))
+        def _(p):
+            give_back(p).wait()
+
+        natural[pl.ds(here, batch), :] = from_wire(
+            swap, returned[pl.ds(here * SUB, batch * SUB), :]
+        )
+        both = dot(picks[stage], natural[pl.ds(here, batch), :])
+        result = rweight[:, :1] * both[:rows] + rweight[:, 1:2] * both[rows:]
+        if stage:
+            result = combined[...] + result
+        if stage < stages - 1:
+            combined[...] = result
+        else:
+            out_ref[...] = result.astype(BF16)
 
 
 def hand_over(mix_ref, out_ref, mix_result, out_result):
@@ -568,7 +578,7 @@
             vmem((tp - 1, slots, width), BF16),
             vmem((slots * SUB, LANE), BF16),
             vmem((slots * SUB, LANE), BF16),
-            vmem((2, top * moe_rows, slots // 2), BF16),
+            vmem((6, top * moe_rows, slots // 6), BF16),
             vmem((moe_rows, width), F32),
             dma(7), dma(tp - 1), dma(tp - 1), dma(ep), dma(ep), dma(tp - 1, 8), dma(tp - 1, 8),
             dma(tp - 1, 2), dma(tp - 1, 2), dma(ep), dma(ep), dma(tp - 1), dma(tp - 1),

time: 225 us -> 221 us (0.982)
  the two profiles are of different devices: /device:TPU:160 before, /device:TPU:33 now
where the time goes in v5:
time: 221 us; the launch traced here: 219 us
  Pallas kernels  218 us (99%)
    pallas_call x1, Pallas kernels, on_device(): pl.pallas_call(functools.partial(kernel, capacity), name='block', out_sha...  216 us

profile of v5, /device:TPU:33, one launch (start us, length us, event | category | flops | bytes accessed | tf_op | source)
XLA Modules:
  0.0 219.0 jit_solution(6390330064697193561)
XLA Ops:
  0.6 216.1 %block.1 = (bf16[128,2048]{1,0:T(8,128)(2,1)}, bf16[128,2048]{1,0:T(8,128)(2,1)}) custom-call(bf16[128,2048]{1,0:T(8,128)(2,1)} %x_ref.1, f32[1,2048]{1,0:T(1,128)} %bitcast.5, bf16[2048,256]{1,0:T(8,128)(2,1)} %wq_ref.1, bf16[2048,256]{1,0:T(8,128)(2,1)} %wk_ref.1, bf16[2048,256]{1,0:T(8,128)(2,1)} %wv_ref.1, bf16[256,2048]{1,0:T(8,128)(2,1)} %wo_ref.1, ...), custom_call_target="tpu_custom_call" | custom-call | tf_op jit(solution)/shard_map/block/pallas_call | solution.py:550
  216.8 2.2 %hand_over.1 = (bf16[128,2048]{1,0:T(8,128)(2,1)}, bf16[128,2048]{1,0:T(8,128)(2,1)}) custom-call(bf16[128,2048]{1,0:T(8,128)(2,1)} %get-tuple-element.4.mix_ref, bf16[128,2048]{1,0:T(8,128)(2,1)} %get-tuple-element.5.out_ref), custom_call_target="tpu_custom_call" | custom-call | tf_op jit(solution)/shard_map/hand_over/pallas_call | solution.py:595
